TPU v7x, 32 devices: a whole 2x2x4 slice. The times are simulated.
32 devices in a mesh: kv: 16 (over z, y, x), tp: 2 (over core).
Axes of the slice: x: 2, y: 2, z: 4, core: 2. Of those that a mesh axis runs over, the one named last changes fastest.
Arguments:
- tokens: bfloat16 [32, 4096], P(None, 'kv'), may hold values from -6 to 6
- norm_gain: bfloat16 [4096], P('kv'), may hold values from 0.099609375 to 1.8984375
- w_query: bfloat16 [4096, 4096], P('kv', 'tp'), may hold values from -0.09375 to 0.09375
- w_key: bfloat16 [4096, 1024], P('kv', 'tp'), may hold values from -0.09375 to 0.09375
- w_value: bfloat16 [4096, 1024], P('kv', 'tp'), may hold values from -0.09375 to 0.09375
- w_forget: bfloat16 [4096, 32], P('kv', 'tp'), may hold values from -0.1875 to 0.1875
- forget_bias: float32 [32], P('tp'), may hold values from -1 to 3
- key_cache: bfloat16 [32, 4096, 1024], P(None, 'kv', 'tp'), may hold values from -1200 to 1200
- value_cache: bfloat16 [32, 4096, 1024], P(None, 'kv', 'tp'), may hold values from -6 to 6
- gate_cache: float32 [32, 32, 4096], P(None, 'tp', 'kv'), may hold values from -515 to 0
- lengths: int32 [32], replicated, may hold values from 1024 to 4095, as said below
- w_out: bfloat16 [4096, 4096], P('tp', 'kv'), may hold values from -0.375 to 0.375
Outputs:
- mixed: bfloat16 [32, 4096], P(None, 'kv')
Inputs may be any that keep to these rules, and one draw needn't show every extreme that they name: `lengths`: at least one sequence has the length 4095 in every draw.
All inputs are finite; a program needn't handle non-finite values.
Results may differ from a plain program's by a relative error of at most 0.018.
Values may be sent and summed in bfloat16 or wider, within the bound.
A program may use at most 64 MiB of HBM per device.

v0:
```python
import jax
import jax.numpy as jnp
from jax import lax
from jax.sharding import PartitionSpec as P

D = 4096
HEAD_DIM = 128


EPSILON = 1e-06
NEGATIVE = -1e30


def joined(value, axis, join):
    pieces = jax.tree.map(lambda part: lax.all_gather(part, axis), value)
    head = jax.tree.map(lambda part: part[0], pieces)
    tail = jax.tree.map(lambda part: part[1:], pieces)
    running, _ = lax.scan(lambda running, piece: (join(running, piece), None), head, tail)
    return running


def combine_parts(earlier, later):
    top_a, total_a, weighted_a = earlier
    top_b, total_b, weighted_b = later
    highest = jnp.maximum(top_a, top_b)
    factor_a = jnp.exp(top_a - highest)
    factor_b = jnp.exp(top_b - highest)
    return (
        highest,
        total_a * factor_a + total_b * factor_b,
        weighted_a * factor_a[..., None] + weighted_b * factor_b[..., None],
    )


def local(
    tokens,
    norm_gain,
    w_query,
    w_key,
    w_value,
    w_forget,
    forget_bias,
    key_cache,
    value_cache,
    gate_cache,
    lengths,
    w_out,
):
    batch_rows = tokens.shape[0]
    head_count = gate_cache.shape[1]
    span = gate_cache.shape[2]
    kv_count = key_cache.shape[2] // HEAD_DIM
    groups = head_count // kv_count
    score_scaling = HEAD_DIM ** (-0.5)
    tokens_f = tokens.astype(jnp.float32)
    squares = jnp.sum(tokens_f * tokens_f, axis=1)
    scaled = (tokens_f * norm_gain.astype(jnp.float32)[None, :]).astype(jnp.bfloat16)
    query_part = jnp.dot(scaled, w_query, preferred_element_type=jnp.float32)
    key_part = jnp.dot(scaled, w_key, preferred_element_type=jnp.float32)
    value_part = jnp.dot(scaled, w_value, preferred_element_type=jnp.float32)
    forget_part = jnp.dot(scaled, w_forget, preferred_element_type=jnp.float32)
    query_sum, key_sum, value_sum, forget_sum, square_sum = lax.psum(
        (query_part, key_part, value_part, forget_part, squares), "kv"
    )
    inverse = lax.rsqrt(square_sum / D + EPSILON)
    query_rows = (
        (query_sum * inverse[:, None])
        .astype(jnp.bfloat16)
        .reshape(batch_rows, kv_count, groups, HEAD_DIM)
    )
    key_rows = key_cache.reshape(batch_rows, span, kv_count, HEAD_DIM)
    scores = jnp.einsum("bkgd,bpkd->bkgp", query_rows, key_rows, preferred_element_type=jnp.float32)
    scores = scores.reshape(batch_rows, head_count, span) * score_scaling + gate_cache
    position = lax.axis_index("kv") * span + lax.broadcasted_iota(jnp.int32, (1, 1, span), 2)
    valid = position < lengths[:, None, None]
    scores = jnp.where(valid, scores, NEGATIVE)
    top_score = jnp.max(scores, axis=2)
    weights = jnp.where(valid, jnp.exp(scores - top_score[..., None]), 0.0)
    total = jnp.sum(weights, axis=2)
    weights_low = weights.astype(jnp.bfloat16).reshape(batch_rows, kv_count, groups, span)
    values = value_cache.reshape(batch_rows, span, kv_count, HEAD_DIM)
    weighted = jnp.einsum(
        "bkgp,bpkd->bkgd", weights_low, values, preferred_element_type=jnp.float32
    )
    weighted = weighted.reshape(batch_rows, head_count, HEAD_DIM)
    top_score, total, weighted = joined((top_score, total, weighted), "kv", combine_parts)
    fresh_key = (
        (key_sum * inverse[:, None]).astype(jnp.bfloat16).reshape(batch_rows, kv_count, HEAD_DIM)
    )
    new_value = (
        (value_sum * inverse[:, None]).astype(jnp.bfloat16).reshape(batch_rows, kv_count, HEAD_DIM)
    )
    forget_logarithm = jax.nn.log_sigmoid(forget_sum * inverse[:, None] + forget_bias[None, :])
    self_token_score = jnp.einsum(
        "cptj,cpj->cpt", query_rows, fresh_key, preferred_element_type=jnp.float32
    )
    self_token_score = (
        self_token_score.reshape(batch_rows, head_count) * score_scaling - forget_logarithm
    )
    highest_all = jnp.maximum(top_score, self_token_score)
    past_factor = jnp.exp(top_score - highest_all)
    own_weight = jnp.exp(self_token_score - highest_all)
    denominator = total * past_factor + own_weight
    own_values = jnp.repeat(new_value.astype(jnp.float32), groups, axis=1)
    attended = (
        weighted * past_factor[..., None] + own_weight[..., None] * own_values
    ) / denominator[..., None]
    attended = attended.astype(jnp.bfloat16).reshape(batch_rows, head_count * HEAD_DIM)
    partial_value = jnp.dot(attended, w_out, preferred_element_type=jnp.float32)
    partial_value = lax.optimization_barrier(partial_value.astype(jnp.bfloat16)).astype(jnp.float32)
    summed = lax.psum(partial_value.astype(jnp.bfloat16), "tp")
    return summed


def solution(mesh):
    in_specs = (
        P(None, "kv"),
        P("kv"),
        P("kv", "tp"),
        P("kv", "tp"),
        P("kv", "tp"),
        P("kv", "tp"),
        P("tp"),
        P(None, "kv", "tp"),
        P(None, "kv", "tp"),
        P(None, "tp", "kv"),
        P(),
        P("tp", "kv"),
    )
    out_specs = P(None, "kv")
    return jax.shard_map(local, mesh=mesh, in_specs=in_specs, out_specs=out_specs, check_vma=False)
```

profile of v0, /device:TPU:0, one launch (start us, length us, event | category | flops | bytes accessed | tf_op | source)
XLA Modules:
  0.0 255.3 jit_solution(1243790228813533830)
XLA Ops:
  6.5 0.8 convert_element_type.36
  7.3 0.5 copy-done
  7.8 1.7 fusion.25
  9.5 1.7 fusion.19
  11.2 1.7 fusion.23
  13.1 0.8 fusion.17
  13.9 0.8 fusion.21
  14.7 44.9 %all-reduce = (f32[32]{0:T(128)S(1)}, f32[32,16]{0,1:T(8,128)S(1)}) all-reduce(f32[32]{0:T(128)S(1)} %fusion.17, f32[32,16]{0,1:T(8,128)S(1)} %fusion.21), channel_id=1, replica_groups=mesh['kv'=16,'tp'=2] {'kv'}, use_global_device_ids=true, to_apply=%region_2.0 | all-reduce | flops 544 | bytes 4352 | tf_op jit(solution)/shard_map/psum | solution.py:62
  59.7 0.7 broadcast_compare_fusion
  60.4 65.2 %all-reduce.4.cloned.1.call-done = (f32[32,512]{1,0:T(8,128)}, f32[32,2048]{1,0:T(8,128)}, f32[32,512]{1,0:T(8,128)}) async-done(((f32[32,512]{1,0:T(8,128)}, f32[32,2048]{1,0:T(8,128)}, f32[32,512]{1,0:T(8,128)}), (f32[32,512]{1,0:T(8,128)}, f32[32,2048]{1,0:T(8,128)}, f32[32,512]{1,0:T(8,128)})) %all-reduce.4.cloned.1.call-update) | async-done | bytes 393232 | tf_op jit(solution)/shard_map/psum | solution.py:62
  125.6 1.0 multiply_convert_fusion
  126.7 5.6 %fusion.9 = f32[32,4,4,256]{3,2,1,0:T(4,128)S(1)} fusion(bf16[32,4,4,128]{3,2,1,0:T(4,128)(2,1)S(1)} %reshape.73, bf16[32,256,512]{2,1,0:T(8,128)(2,1)} %param.21), kind=kOutput, calls=%fused_computation.14 | convolution fusion | flops 33685504 | bytes 9043968 | tf_op jit(solution)/shard_map/bkgd,bpkd->bkgp/dot_general | solution.py:72
  132.3 0.2 mul.111
  132.5 0.1 fusion.31
  132.7 0.3 fusion.12
  133.1 5.3 %fusion.3 = f32[32,4,4,128]{3,2,1,0:T(4,128)} fusion(bf16[32,4,4,256]{3,2,1,0:T(4,128)(2,1)S(1)} %reshape.75, bf16[32,256,512]{2,1,0:T(8,128)(2,1)} %param.22), kind=kOutput, calls=%fused_computation.8 | convolution fusion | flops 33554432 | bytes 8912896 | tf_op jit(solution)/shard_map/bkgp,bpkd->bkgd/dot_general | solution.py:82
  138.4 40.2 %all-gather.3 = f32[16,32,16]{1,2,0:T(8,128)S(1)} all-gather(f32[1,32,16]{1,2,0:T(8,128)S(1)} %copy.25), channel_id=3, replica_groups=mesh['kv'=16,'tp'=2] {'kv'}, dimensions={0}, use_global_device_ids=true | all-gather | bytes 34816 | tf_op jit(solution)/shard_map/all_gather | solution.py:15
  178.7 37.7 %all-gather.2 = f32[16,32,16]{1,2,0:T(8,128)S(1)} all-gather(f32[1,32,16]{1,2,0:T(8,128)S(1)} %copy.24), channel_id=2, replica_groups=mesh['kv'=16,'tp'=2] {'kv'}, dimensions={0}, use_global_device_ids=true | all-gather | bytes 34816 | tf_op jit(solution)/shard_map/all_gather | solution.py:15
  216.4 0.1 multiply_convert_fusion.2
  216.5 0.3 fusion.35
  216.8 0.1 copy.31
  217.0 4.3 %slice.37 = f32[15,32,16,128]{3,2,1,0:T(8,128)} slice(f32[16,32,16,128]{3,2,1,0:T(8,128)} %all-gather.6.cloned.1.call-done), slice={[1:16], [0:32], [0:16], [0:128]} | slice | bytes 7864320 | tf_op jit(solution)/shard_map/slice | solution.py:17
  221.4 1.0 slice_bitcast_fusion
  222.3 21.2 %while.14 = (s32[]{:T(128)}, f32[32,16]{0,1:T(8,128)S(1)}, f32[32,16]{0,1:T(8,128)S(1)}, f32[32,16,128]{2,1,0:T(8,128)S(1)}, f32[15,32,16]{1,2,0:T(8,128)S(1)}, ...) while((s32[]{:T(128)}, f32[32,16]{0,1:T(8,128)S(1)}, f32[32,16]{0,1:T(8,128)S(1)}, ...), condition=%wide.region_6.7_spmd, body=%wide.region_5.0_spmd.sunk | while | flops 199682 | bytes 815197 | solution.py:18
  222.4 0.1 copy.51
  222.5 1.2 fusion.50
  223.9 1.2 fusion.50
  225.2 0.1 copy.51
  225.4 1.2 fusion.50
  226.6 0.1 copy.51
  226.8 1.2 fusion.50
  228.0 0.1 copy.51
  228.2 1.2 fusion.50
  229.4 0.1 copy.51
  229.6 1.2 fusion.50
  231.0 1.2 fusion.50
  232.4 1.2 fusion.50
  233.8 1.2 fusion.50
  235.3 1.2 fusion.50
  236.7 1.2 fusion.50
  238.1 1.2 fusion.50
  239.5 1.2 fusion.50
  240.9 1.2 fusion.50
  242.3 1.2 fusion.50
  243.6 0.1 multiply_add_fusion
  244.0 0.3 divide_convert_fusion
  244.3 0.3 convolution_convert_fusion
  244.5 4.0 %psum.47 = bf16[32,256]{1,0:T(8,128)(2,1)} all-reduce(bf16[32,256]{1,0:T(8,128)(2,1)S(1)} %convolution_convert_fusion), channel_id=1, replica_groups=mesh['kv'=16,'tp'=2] {'tp'}, use_global_device_ids=true, to_apply=%region_10.11 | all-reduce | flops 8192 | bytes 32768 | tf_op jit(solution)/shard_map/psum | solution.py:111
  (73 shorter events, 2.9 us)
Async XLA Ops:
  6.5 1.2 copy-start
  6.5 126.0 %copy-start.1 = (f32[32,16,256]{2,1,0:T(8,128)S(1)}, f32[32,16,256]{2,1,0:T(8,128)}, u32[]{:S(2)}) copy-start(f32[32,16,256]{2,1,0:T(8,128)} %param.23) | copy-start | bytes 1572868
  6.5 119.0 %all-reduce.4.cloned.1.call-start = ((), (), s32[]{:S(2)}) async-start(), calls=%async_computation.1 | async-start | bytes 786432 | tf_op jit(solution)/shard_map/psum | solution.py:62
  13.0 204.0 %all-gather.6.cloned.1.call-start = ((), (), s32[]{:S(2)}) async-start(), calls=%async_computation | async-start | bytes 4456448 | tf_op jit(solution)/shard_map/all_gather | solution.py:15
  132.3 84.1 %copy-start.3 = (f32[32,512]{1,0:T(8,128)S(1)}, f32[32,512]{1,0:T(8,128)}, u32[]{:S(2)}) copy-start(f32[32,512]{1,0:T(8,128)} %get-tuple-element.63) | copy-start | bytes 196612
  132.3 84.1 %copy-start.4 = (f32[32,512]{1,0:T(8,128)S(1)}, f32[32,512]{1,0:T(8,128)}, u32[]{:S(2)}) copy-start(f32[32,512]{1,0:T(8,128)} %get-tuple-element.65) | copy-start | bytes 196612
  138.3 105.2 %copy-start.5 = (f32[16]{0:T(128)S(1)}, f32[16]{0:T(128)}, u32[]{:S(2)}) copy-start(f32[16]{0:T(128)} %param.20) | copy-start | bytes 196
  138.3 105.9 %copy-start.2 = (bf16[2048,256]{1,0:T(8,128)(2,1)S(1)}, bf16[2048,256]{1,0:T(8,128)(2,1)}, u32[]{:S(2)}) copy-start(bf16[2048,256]{1,0:T(8,128)(2,1)} %param.25) | copy-start | bytes 3145732
Sparse Core Ops, SparseCore 0:
  13.1 112.3 all-reduce.3
  138.5 75.5 all-gather.5
where the time goes:
time: 256 us; the launch traced here: 255 us
  blocking collectives  127 us (50%)
  waiting for transfers between devices  65.2 us (25%)
  other arithmetic  22.9 us (9%)
  matrix products  17.5 us (7%)
  between operations  13.6 us (5%)
  local copies, waits for them, and re-layouts  8.93 us (3%)
    all_gather x2, blocking collectives, joined(): pieces = jax.tree.map(lambda part: lax.all_gather(part, axis), value)  77.9 us
    psum x1, waiting for transfers between devices, local(): lax.psum((query_part, key_part, value_part, forget_part, squares), 'kv')  65.2 us
    psum x1, blocking collectives, local(): lax.psum((query_part, key_part, value_part, forget_part, squares), 'kv')  44.9 us
    add x15, other arithmetic, combine_parts(): weighted_a * factor_a[..., None] + weighted_b * factor_b[..., None]  18.3 us
    dot_general x1, matrix products, local(): jnp.einsum('bkgd,bpkd->bkgp', query_rows, key_rows, preferred_element_typ...  5.64 us
    dot_general x1, matrix products, local(): jnp.einsum('bkgp,bpkd->bkgd', weights_low, values, preferred_element_type...  5.27 us
  transfers between devices with their start and end apart: 2, of which 1 were waited for; matrix products, arithmetic and copies ran while one was open for 1% of the time, Pallas kernels for 0%

commit v1 on v0

v1 whole, which is shorter than its diff:
```python
import functools

import jax
import jax.numpy as jnp
from jax import lax
from jax.experimental import pallas as pl
from jax.experimental.pallas import tpu as pltpu
from jax.sharding import PartitionSpec as P

HEAD_DIM = 128
EPSILON = 1e-06
NEGATIVE = -1e30
ROWS = 8
PARTS = 8
F32 = jnp.float32
BF16 = jnp.bfloat16


def iota(shape, dim):
    return lax.broadcasted_iota(jnp.int32, shape, dim)


def one_hot(condition):
    return jnp.where(condition, 1.0, 0.0).astype(BF16)


def dot(a, b):
    return jnp.dot(a, b, preferred_element_type=F32)


def round_low(x):
    return x.astype(BF16).astype(F32)


def split3(x):
    high = round_low(x)
    rest = x - high
    mid = round_low(rest)
    return high, mid, round_low(rest - mid)


def kernel(
    n, tp, heads, kv_count, batch, span, width,
    tokens_ref, gain_ref, bias_ref, lengths_ref,
    wq_hbm, wk_hbm, wv_hbm, wf_ref, k_hbm, v_hbm, gate_hbm, wo_hbm,
    out_ref,
    wq, wk, wv, kbuf, vbuf, gate, wo,
    send1, recv1, qbuf, send2, recv2, stat, att, pair,
    wsem, ksem, vsem, gsem,
    s1, r1, s2, r2, s3, r3, s4, r4, s5, r5,
):
    me = lax.axis_index("kv")
    my_tp = lax.axis_index("tp")
    groups = heads // kv_count
    row_groups = batch // ROWS
    units = row_groups * kv_count
    stride = n // units
    qcols = groups * HEAD_DIM
    unit_rows = groups * ROWS
    scale = HEAD_DIM ** (-0.5)
    my_unit = me // stride
    my_r = my_unit // kv_count
    my_g = my_unit % kv_count
    is_owner = (me % stride) == 0

    def owner_only(body):
        if stride == 1:
            body()
        else:
            pl.when(is_owner)(body)

    barrier = pltpu.get_barrier_semaphore()

    def greet(k, carry):
        pl.semaphore_signal(
            barrier, inc=1, device_id={"kv": lax.rem(me + k, n)},
            device_id_type=pl.DeviceIdType.MESH,
        )
        return carry

    lax.fori_loop(1, n, greet, 0)
    for k in range(1, tp):
        pl.semaphore_signal(
            barrier, inc=1, device_id={"tp": lax.rem(my_tp + k, tp)},
            device_id_type=pl.DeviceIdType.MESH,
        )

    w_copies = [
        pltpu.make_async_copy(src, dst, wsem.at[i])
        for i, (src, dst) in enumerate(((wq_hbm, wq), (wk_hbm, wk), (wv_hbm, wv)))
    ]
    wo_copy = pltpu.make_async_copy(wo_hbm, wo, wsem.at[3])
    gate_copy = pltpu.make_async_copy(gate_hbm, gate, gsem)
    for c in w_copies:
        c.start()

    def cache_copy(hbm, buf, sems, r):
        rows = pl.ds(pl.multiple_of(r * ROWS, ROWS), ROWS)
        return pltpu.make_async_copy(hbm.at[rows], buf.at[rows], sems.at[r])

    tokens_f = tokens_ref[...].astype(F32)
    squares = jnp.sum(tokens_f * tokens_f, axis=1, keepdims=True)
    scaled = (tokens_f * gain_ref[...].astype(F32)).astype(BF16)
    forget = dot(scaled, wf_ref[...])
    lane = iota((batch, HEAD_DIM), 1)
    fh = round_low(forget)
    fl = forget - fh
    place_r = iota((heads, HEAD_DIM), 0)
    place_c = iota((heads, HEAD_DIM), 1)
    sh, sm, sl = split3(squares)
    extra = (
        dot(fh.astype(BF16), one_hot(place_c == place_r))
        + dot(fl.astype(BF16), one_hot(place_c == place_r + heads))
        + jnp.where(lane == 2 * heads, sh, 0.0)
        + jnp.where(lane == 2 * heads + 1, sm, 0.0)
        + jnp.where(lane == 2 * heads + 2, sl, 0.0)
    )
    for c in w_copies:
        c.wait()
    for k in range(row_groups):
        r = lax.rem(my_r + k, row_groups)
        cache_copy(k_hbm, kbuf, ksem, r).start()
        if k == 0:
            gate_copy.start()
        cache_copy(v_hbm, vbuf, vsem, r).start()
    wo_copy.start()

    for g in range(kv_count):
        qg = dot(scaled, wq[:, g * qcols:(g + 1) * qcols])
        kg = dot(scaled, wk[:, g * HEAD_DIM:(g + 1) * HEAD_DIM])
        vg = dot(scaled, wv[:, g * HEAD_DIM:(g + 1) * HEAD_DIM])
        for r in range(row_groups):
            at = slice(r * ROWS, (r + 1) * ROWS)
            u = r * kv_count + g
            send1[u, :, 0:qcols] = qg[at].astype(BF16)
            send1[u, :, qcols:qcols + HEAD_DIM] = kg[at].astype(BF16)
            send1[u, :, qcols + HEAD_DIM:qcols + 2 * HEAD_DIM] = vg[at].astype(BF16)
            send1[u, :, qcols + 2 * HEAD_DIM:qcols + 3 * HEAD_DIM] = extra[at].astype(BF16)

    pl.semaphore_wait(barrier, n - 1 + tp - 1)

    def rs1(u):
        return pltpu.make_async_remote_copy(
            src_ref=send1.at[u], dst_ref=recv1.at[me], send_sem=s1.at[u],
            recv_sem=r1.at[me], device_id={"kv": u * stride},
            device_id_type=pl.DeviceIdType.MESH,
        )

    def rs1_from(d):
        return pltpu.make_async_remote_copy(
            src_ref=send1.at[0], dst_ref=recv1.at[d], send_sem=s1.at[0],
            recv_sem=r1.at[d], device_id={"kv": me}, device_id_type=pl.DeviceIdType.MESH,
        )

    def start_rs1(k, carry):
        u = lax.rem(my_unit + k, units)

        @pl.when(u * stride != me)
        def _():
            rs1(u).start()
        return carry

    lax.fori_loop(0, units, start_rs1, 0)

    def ag1(u, d):
        return pltpu.make_async_remote_copy(
            src_ref=qbuf.at[u], dst_ref=qbuf.at[u], send_sem=s2.at[d],
            recv_sem=r2.at[u], device_id={"kv": d}, device_id_type=pl.DeviceIdType.MESH,
        )

    own_parts = {}

    def project():
        total0 = send1[my_unit].astype(F32)

        def add(k, acc):
            d = lax.rem(me + k, n)
            rs1_from(d).wait_recv()
            return acc + recv1[d].astype(F32)

        sums = lax.fori_loop(1, n, add, total0)
        fs = sums[:, qcols + 2 * HEAD_DIM:]
        fl8 = iota((ROWS, HEAD_DIM), 1)

        def pick(mask):
            return jnp.sum(jnp.where(mask, fs, 0.0), axis=1, keepdims=True)

        square = pick((fl8 >= 2 * heads) & (fl8 <= 2 * heads + 2))
        inverse = lax.rsqrt(square / width + EPSILON)
        query = round_low(sums[:, :qcols] * inverse)
        by_head = [query[:, h * HEAD_DIM:(h + 1) * HEAD_DIM] for h in range(groups)]
        qbuf[my_unit] = jnp.concatenate(by_head, axis=0).astype(BF16)

        def send(k, carry):
            ag1(my_unit, lax.rem(me + k, n)).start()
            return carry

        lax.fori_loop(1, n, send, 0)
        new_key = round_low(sums[:, qcols:qcols + HEAD_DIM] * inverse)
        new_value = round_low(sums[:, qcols + HEAD_DIM:qcols + 2 * HEAD_DIM] * inverse)
        owns = []
        for h in range(groups):
            head = my_g * groups + h
            x = pick((fl8 == head) | (fl8 == head + heads)) * inverse + bias_ref[head]
            softplus = jnp.maximum(-x, 0.0) + jnp.log1p(jnp.exp(-jnp.abs(x)))
            score = jnp.sum(by_head[h] * new_key, axis=1, keepdims=True) * scale + softplus
            owns.append(jnp.broadcast_to(score, (ROWS, HEAD_DIM)))
        own_parts["score"] = jnp.concatenate(owns, axis=1)
        own_parts["value"] = new_value
        pair_own[0] = own_parts["score"]
        pair_own[1] = jnp.concatenate([new_value] * groups, axis=1)

    pair_own = stat["own"]
    owner_only(project)

    gate_copy.wait()
    m_rows = ROWS * heads

    def rs2(u):
        return pltpu.make_async_remote_copy(
            src_ref=send2.at[u], dst_ref=recv2.at[me], send_sem=s3.at[u],
            recv_sem=r3.at[me], device_id={"kv": u * stride},
            device_id_type=pl.DeviceIdType.MESH,
        )

    def rs2_from(d):
        return pltpu.make_async_remote_copy(
            src_ref=send2.at[0], dst_ref=recv2.at[d], send_sem=s3.at[0],
            recv_sem=r3.at[d], device_id={"kv": me}, device_id_type=pl.DeviceIdType.MESH,
        )

    def ag1_from(u):
        return ag1(u, me)

    def attend(step, carry):
        r = lax.rem(my_r + step, row_groups)
        si = iota((m_rows, unit_rows), 0)
        sj = iota((m_rows, unit_rows), 1)
        blocks = []
        for g in range(kv_count):
            u = r * kv_count + g

            @pl.when(u * stride != me)
            def _():
                ag1_from(u).wait_recv()
            source = (si % heads - g * groups) * ROWS + si // heads
            inside = (si % heads) // groups == g
            blocks.append(dot(one_hot(inside & (sj == source)), qbuf[u]).astype(BF16))
        queries = jnp.concatenate(blocks, axis=1)
        cache_copy(k_hbm, kbuf, ksem, r).wait()
        position = me * span + iota((heads, span), 1)
        scores, valids = [], []
        for b in range(ROWS):
            row = r * ROWS + b
            s = lax.dot_general(
                queries[b * heads:(b + 1) * heads], kbuf[row],
                (((1,), (1,)), ((), ())), preferred_element_type=F32,
            )
            s = s * scale + gate[row]
            valid = position < lengths_ref[row]
            scores.append(jnp.where(valid, s, NEGATIVE))
            valids.append(jnp.where(valid, 1.0, 0.0))
        score = jnp.concatenate(scores, axis=0)
        kept = jnp.concatenate(valids, axis=0) > 0.0
        top = jnp.max(score, axis=1, keepdims=True)
        weight = jnp.where(kept, jnp.exp(score - top), 0.0)
        total = jnp.sum(weight, axis=1, keepdims=True)
        low = weight.astype(BF16)
        cache_copy(v_hbm, vbuf, vsem, r).wait()
        values = []
        head_group = iota((heads, HEAD_DIM), 0) // groups
        for b in range(ROWS):
            full = dot(low[b * heads:(b + 1) * heads], vbuf[r * ROWS + b])
            mine = full[:, :HEAD_DIM]
            for g in range(1, kv_count):
                mine = jnp.where(head_group == g, full[:, g * HEAD_DIM:(g + 1) * HEAD_DIM], mine)
            values.append(mine.astype(BF16))
        value = jnp.concatenate(values, axis=0)

        li = iota((m_rows, HEAD_DIM), 0)
        ll = iota((m_rows, HEAD_DIM), 1)
        here = ll // PARTS == li % groups

        def spread(x):
            a, b, c = split3(x)
            part = ll % PARTS
            picked = jnp.where(part == 0, a, jnp.where(part == 1, b, jnp.where(part == 2, c, 0.0)))
            return jnp.where(here, picked, 0.0).astype(BF16)

        ti = iota((m_rows, m_rows), 0)
        tj = iota((m_rows, m_rows), 1)
        moved = dot(one_hot(tj == (ti % ROWS) * heads + ti // ROWS), value).astype(BF16)
        wi = iota((kv_count * ROWS, m_rows), 0)
        wj = iota((kv_count * ROWS, m_rows), 1)
        gather = one_hot((wj // heads == wi % ROWS) & ((wj % heads) // groups == wi // ROWS))
        tops = dot(gather, spread(top))
        totals = dot(gather, spread(total))
        for g in range(kv_count):
            u = r * kv_count + g
            at = slice(g * ROWS, (g + 1) * ROWS)
            send2[u, 0:unit_rows] = moved[g * unit_rows:(g + 1) * unit_rows]
            send2[u, unit_rows:unit_rows + 2 * ROWS] = jnp.concatenate(
                [tops[at], totals[at]], axis=0
            ).astype(BF16)

            @pl.when(u * stride != me)
            def _():
                rs2(u).start()
        return carry

    lax.fori_loop(0, row_groups, attend, 0)

    def ag2(u, d):
        return pltpu.make_async_remote_copy(
            src_ref=att.at[u], dst_ref=att.at[u], send_sem=s4.at[d],
            recv_sem=r4.at[u], device_id={"kv": d}, device_id_type=pl.DeviceIdType.MESH,
        )

    def slot(u):
        return lax.rem(u, kv_count) * row_groups + u // kv_count

    def join():
        recv2[me] = send2[my_unit]

        def arrived(k, carry):
            rs2_from(lax.rem(me + k, n)).wait_recv()
            return carry

        lax.fori_loop(1, n, arrived, 0)
        ei = iota((HEAD_DIM, qcols), 0)
        ej = iota((HEAD_DIM, qcols), 1)
        widen = one_hot((ei // PARTS == ej // HEAD_DIM) & (ei % PARTS < 3))
        packed = recv2[:, unit_rows:unit_rows + 2 * ROWS, :].reshape(n * 2 * ROWS, HEAD_DIM)
        stat["all"][...] = dot(packed, widen).reshape(n, 2 * ROWS, qcols)
        own = pair_own[0]

        def highest(d, top):
            return jnp.maximum(top, stat["all"][d, 0:ROWS])

        top = lax.fori_loop(0, n, highest, own, unroll=4)

        def gather(d, carry):
            total, acc = carry
            factor = jnp.exp(stat["all"][d, 0:ROWS] - top)
            piece = recv2[d, 0:unit_rows].astype(F32)
            piece = jnp.concatenate(
                [piece[h * ROWS:(h + 1) * ROWS] for h in range(groups)], axis=1
            )
            return total + stat["all"][d, ROWS:2 * ROWS] * factor, acc + piece * factor

        own_weight = jnp.exp(own - top)
        total, acc = lax.fori_loop(
            0, n, gather, (own_weight, own_weight * pair_own[1]), unroll=4
        )
        att[slot(my_unit)] = (acc / total).astype(BF16)

        def send(k, carry):
            ag2(slot(my_unit), lax.rem(me + k, n)).start()
            return carry

        lax.fori_loop(1, n, send, 0)

    owner_only(join)

    wo_copy.wait()
    part = None
    for g in range(kv_count):
        for r in range(row_groups):
            @pl.when((r * kv_count + g) * stride != me)
            def _():
                ag2(g * row_groups + r, me).wait_recv()
        rows = att[g * row_groups:(g + 1) * row_groups].astype(F32).reshape(batch, qcols).astype(BF16)
        term = dot(rows, wo[g * qcols:(g + 1) * qcols, :])
        part = term if part is None else part + term

    pair[my_tp] = part.astype(BF16)
    exchanges = []
    for k in range(1, tp):
        c = pltpu.make_async_remote_copy(
            src_ref=pair.at[my_tp], dst_ref=pair.at[my_tp], send_sem=s5.at[k],
            recv_sem=r5.at[my_tp], device_id={"tp": lax.rem(my_tp + k, tp)},
            device_id_type=pl.DeviceIdType.MESH,
        )
        c.start()
        exchanges.append(c)
    for k in range(1, tp):
        other = lax.rem(my_tp + k, tp)
        pltpu.make_async_remote_copy(
            src_ref=pair.at[other], dst_ref=pair.at[other], send_sem=s5.at[k],
            recv_sem=r5.at[other], device_id={"tp": my_tp},
            device_id_type=pl.DeviceIdType.MESH,
        ).wait_recv()
    summed = pair[0].astype(F32)
    for k in range(1, tp):
        summed = summed + pair[k].astype(F32)
    out_ref[...] = summed

    def drain_units(u, carry):
        @pl.when(u * stride != me)
        def _():
            rs1(u).wait_send()
            rs2(u).wait_send()
        return carry

    lax.fori_loop(0, units, drain_units, 0)

    def drain_owner():
        def drain(k, carry):
            d = lax.rem(me + k, n)
            ag1(my_unit, d).wait_send()
            ag2(slot(my_unit), d).wait_send()
            return carry

        lax.fori_loop(1, n, drain, 0)

    owner_only(drain_owner)
    for c in exchanges:
        c.wait_send()


def solution(mesh):
    n, tp = mesh.shape["kv"], mesh.shape["tp"]

    def local(
        tokens, norm_gain, w_query, w_key, w_value, w_forget, forget_bias,
        key_cache, value_cache, gate_cache, lengths, w_out,
    ):
        batch, depth = tokens.shape
        heads, span = gate_cache.shape[1], gate_cache.shape[2]
        kv_count = key_cache.shape[2] // HEAD_DIM
        groups = heads // kv_count
        qcols = groups * HEAD_DIM
        units = batch // ROWS * kv_count
        assert n % units == 0
        out_cols = w_out.shape[1]
        vmem = pl.BlockSpec(memory_space=pltpu.VMEM)
        smem = pl.BlockSpec(memory_space=pltpu.SMEM)
        hbm = pl.BlockSpec(memory_space=pl.ANY)
        dma = pltpu.SemaphoreType.DMA
        body = functools.partial(
            kernel, n, tp, heads, kv_count, batch, span, float(n * depth)
        )
        summed = pl.pallas_call(
            body,
            out_shape=jax.ShapeDtypeStruct((batch, out_cols), F32),
            in_specs=[vmem, vmem, smem, smem, hbm, hbm, hbm, vmem, hbm, hbm, hbm, hbm],
            out_specs=vmem,
            scratch_shapes=[
                pltpu.VMEM(w_query.shape, BF16),
                pltpu.VMEM(w_key.shape, BF16),
                pltpu.VMEM(w_value.shape, BF16),
                pltpu.VMEM(key_cache.shape, BF16),
                pltpu.VMEM(value_cache.shape, BF16),
                pltpu.VMEM(gate_cache.shape, F32),
                pltpu.VMEM(w_out.shape, BF16),
                pltpu.VMEM((units, ROWS, qcols + 3 * HEAD_DIM), BF16),
                pltpu.VMEM((n, ROWS, qcols + 3 * HEAD_DIM), BF16),
                pltpu.VMEM((units, groups * ROWS, HEAD_DIM), BF16),
                pltpu.VMEM((units, (groups + 2) * ROWS, HEAD_DIM), BF16),
                pltpu.VMEM((n, (groups + 2) * ROWS, HEAD_DIM), BF16),
                {
                    "all": pltpu.VMEM((n, 2 * ROWS, qcols), F32),
                    "own": pltpu.VMEM((2, ROWS, qcols), F32),
                },
                pltpu.VMEM((units, ROWS, qcols), BF16),
                pltpu.VMEM((tp, batch, out_cols), BF16),
                dma((4,)), dma((batch // ROWS,)), dma((batch // ROWS,)), dma,
                dma((units,)), dma((n,)), dma((n,)), dma((units,)),
                dma((units,)), dma((n,)), dma((n,)), dma((units,)),
                dma((tp,)), dma((tp,)),
            ],
            compiler_params=pltpu.CompilerParams(
                collective_id=0, has_side_effects=True, vmem_limit_bytes=48 * 2**20
            ),
        )(
            tokens, norm_gain.reshape(1, depth), forget_bias, lengths,
            w_query, w_key, w_value, w_forget, key_cache, value_cache, gate_cache, w_out,
        )
        return summed.astype(BF16)

    in_specs = (
        P(None, "kv"), P("kv"), P("kv", "tp"), P("kv", "tp"), P("kv", "tp"),
        P("kv", "tp"), P("tp"), P(None, "kv", "tp"), P(None, "kv", "tp"),
        P(None, "tp", "kv"), P(), P("tp", "kv"),
    )
    return jax.shard_map(
        local, mesh=mesh, in_specs=in_specs, out_specs=P(None, "kv"), check_vma=False
    )
```

time: 256 us -> 46.9 us (0.18)
  blocking collectives: 127 us -> 0 us
  waiting for transfers between devices: 65.2 us -> 0 us
  Pallas kernels: 0 us -> 36.9 us
  other arithmetic: 22.9 us -> 0.61 us
  matrix products: 17.5 us -> 0 us
  between operations: 13.6 us -> 0.02 us
    all_gather x2 -> x0, blocking collectives: 77.9 us -> none  [joined(): pieces = jax.tree.map(lambda part: lax.all_gather(part, axis), value)]
    psum x1 -> x0, waiting for transfers between devices: 65.2 us -> none  [local(): lax.psum((query_part, key_part, value_part, forget_part, squares), 'kv')]
    psum x2 -> x0, blocking collectives: 48.9 us -> none  [the longest x1 44.9 us: local(): lax.psum((query_part, key_part, value_part, forget_part, squares), 'kv')]
    pallas_call x0 -> x1, Pallas kernels: none -> 36.9 us  [local(): pl.pallas_call(body, out_shape=jax.ShapeDtypeStruct((batch, out_cols), F3...]
    add x32 -> x0, other arithmetic: 18.7 us -> none  [the longest x15 18.3 us: combine_parts(): weighted_a * factor_a[..., None] + weighted_b * factor_b[..., None]]
    dot_general x8 -> x0, matrix products: 17.5 us -> none  [the longest x1 5.64 us: local(): jnp.einsum('bkgd,bpkd->bkgp', query_rows, key_rows, preferred_element_typ...]
    unnamed x14 -> x17, local copies, waits for them, and re-layouts: 0.61 us -> 8.23 us
    slice x5 -> x0, local copies, waits for them, and re-layouts: 4.36 us -> none  [the longest x3 4.35 us: joined(): tail = jax.tree.map(lambda part: part[1:], pieces)]
  transfers between devices with their start and end apart: 2 -> 0, of which waited for: 1 -> 0; matrix products, arithmetic and copies ran while one was open for 1% -> 0% of each run, Pallas kernels for 0% -> 0%
where the time goes in v1:
time: 46.9 us; the launch traced here: 46.4 us
  Pallas kernels  36.9 us (79%)
  local copies, waits for them, and re-layouts  8.89 us (19%)
  other arithmetic  0.61 us (1%)
    pallas_call x1, Pallas kernels, local(): pl.pallas_call(body, out_shape=jax.ShapeDtypeStruct((batch, out_cols), F3...  36.9 us
    unnamed x17, local copies, waits for them, and re-layouts  8.23 us

profile of v1, /device:TPU:0, one launch (start us, length us, event | category | flops | bytes accessed | tf_op | source)
XLA Modules:
  0.0 46.4 jit_solution(10769926896472514489)
XLA Ops:
  0.0 0.7 %reshape.3.gain_ref = bf16[1,256]{1,0:T(2,128)(2,1)S(1)} reshape(bf16[256]{0:T(256)(128)(2,1)} %param.13) | data formatting | bytes 1024 | tf_op jit(solution)/shard_map/reshape | solution.py:476
  0.7 0.8 %copy.13.wf_ref = bf16[256,16]{1,0:T(8,128)(2,1)S(1)} copy(bf16[256,16]{0,1:T(8,128)(2,1)} %param.17) | data formatting | bytes 16384 | tf_op args[5]
  1.5 0.0 copy-start
  1.5 1.2 %copy-done = bf16[256,2048]{1,0:T(8,128)(2,1)S(1)} copy-done((bf16[256,2048]{1,0:T(8,128)(2,1)S(1)}, bf16[256,2048]{1,0:T(8,128)(2,1)}, u32[]{:S(2)}) %copy-start) | copy-done | bytes 1048600
  2.7 0.0 copy-start.1
  2.7 1.2 %copy-done.1 = bf16[2048,256]{1,0:T(8,128)(2,1)S(1)} copy-done((bf16[2048,256]{1,0:T(8,128)(2,1)S(1)}, bf16[2048,256]{1,0:T(8,128)(2,1)}, u32[]{:S(2)}) %copy-start.1) | copy-done | bytes 1048600
  3.9 0.0 copy-start.2
  3.9 1.0 %copy-done.2 = f32[32,16,256]{2,1,0:T(8,128)S(1)} copy-done((f32[32,16,256]{2,1,0:T(8,128)S(1)}, f32[32,16,256]{2,1,0:T(8,128)}, u32[]{:S(2)}) %copy-start.2) | copy-done | bytes 524312
  5.0 0.0 copy-start.3
  5.0 0.9 %copy-done.3 = bf16[256,512]{1,0:T(8,128)(2,1)S(1)} copy-done((bf16[256,512]{1,0:T(8,128)(2,1)S(1)}, bf16[256,512]{1,0:T(8,128)(2,1)}, u32[]{:S(2)}) %copy-start.3) | copy-done | bytes 262168
  5.9 0.0 copy-start.4
  5.9 0.9 %copy-done.4 = bf16[256,512]{1,0:T(8,128)(2,1)S(1)} copy-done((bf16[256,512]{1,0:T(8,128)(2,1)S(1)}, bf16[256,512]{1,0:T(8,128)(2,1)}, u32[]{:S(2)}) %copy-start.4) | copy-done | bytes 262168
  6.9 0.0 copy-start.5
  6.9 0.7 %copy-done.5 = bf16[32,256]{1,0:T(8,128)(2,1)S(1)} copy-done((bf16[32,256]{1,0:T(8,128)(2,1)S(1)}, bf16[32,256]{1,0:T(8,128)(2,1)}, u32[]{:S(2)}) %copy-start.5) | copy-done | bytes 16408
  7.6 0.0 copy-start.6
  7.6 0.7 %copy-done.6 = f32[16]{0:T(128)S(1)} copy-done((f32[16]{0:T(128)S(1)}, f32[16]{0:T(128)}, u32[]{:S(2)}) %copy-start.6) | copy-done | bytes 88
  8.2 0.0 copy-start.7
  8.2 0.7 %copy-done.7 = s32[32]{0:T(128)S(1)} copy-done((s32[32]{0:T(128)S(1)}, s32[32]{0:T(128)}, u32[]{:S(2)}) %copy-start.7) | copy-done | bytes 152
  8.9 36.9 %shard_map.118 = f32[32,256]{1,0:T(8,128)S(1)} custom-call(bf16[32,256]{1,0:T(8,128)(2,1)S(1)} %copy-done.5, bf16[1,256]{1,0:T(2,128)(2,1)S(1)} %reshape.3.gain_ref, f32[16]{0:T(128)S(1)} %copy-done.6, s32[32]{0:T(128)S(1)} %copy-done.7, bf16[256,2048]{1,0:T(8,128)(2,1)S(1)} %copy-done, bf16[256,512]{1,0:T(8,128)(2,1)S(1)} %copy-done.3, ...), custom_call_target="tpu_custom_call" | custom-call | tf_op jit(solution)/shard_map/pallas_call | solution.py:443
  45.8 0.6 %convert_element_type.3 = bf16[32,256]{1,0:T(8,128)(2,1)} convert(f32[32,256]{1,0:T(8,128)S(1)} %shard_map.118) | non-fusion elementwise | flops 8192 | bytes 49152 | tf_op jit(solution)/shard_map/convert_element_type | solution.py:479
Async XLA Ops:
  1.5 1.2 %copy-start = (bf16[256,2048]{1,0:T(8,128)(2,1)S(1)}, bf16[256,2048]{1,0:T(8,128)(2,1)}, u32[]{:S(2)}) copy-start(bf16[256,2048]{1,0:T(8,128)(2,1)} %wq_hbm.1) | copy-start | bytes 3145732
  2.7 1.2 %copy-start.1 = (bf16[2048,256]{1,0:T(8,128)(2,1)S(1)}, bf16[2048,256]{1,0:T(8,128)(2,1)}, u32[]{:S(2)}) copy-start(bf16[2048,256]{1,0:T(8,128)(2,1)} %wo_hbm.1) | copy-start | bytes 3145732
  3.9 1.0 %copy-start.2 = (f32[32,16,256]{2,1,0:T(8,128)S(1)}, f32[32,16,256]{2,1,0:T(8,128)}, u32[]{:S(2)}) copy-start(f32[32,16,256]{2,1,0:T(8,128)} %gate_hbm.1) | copy-start | bytes 1572868
  5.0 0.9 %copy-start.3 = (bf16[256,512]{1,0:T(8,128)(2,1)S(1)}, bf16[256,512]{1,0:T(8,128)(2,1)}, u32[]{:S(2)}) copy-start(bf16[256,512]{1,0:T(8,128)(2,1)} %wk_hbm.1) | copy-start | bytes 786436
  5.9 0.9 %copy-start.4 = (bf16[256,512]{1,0:T(8,128)(2,1)S(1)}, bf16[256,512]{1,0:T(8,128)(2,1)}, u32[]{:S(2)}) copy-start(bf16[256,512]{1,0:T(8,128)(2,1)} %wv_hbm.1) | copy-start | bytes 786436
  6.9 0.7 %copy-start.5 = (bf16[32,256]{1,0:T(8,128)(2,1)S(1)}, bf16[32,256]{1,0:T(8,128)(2,1)}, u32[]{:S(2)}) copy-start(bf16[32,256]{1,0:T(8,128)(2,1)} %tokens_ref.1) | copy-start | bytes 49156
  7.6 0.7 %copy-start.6 = (f32[16]{0:T(128)S(1)}, f32[16]{0:T(128)}, u32[]{:S(2)}) copy-start(f32[16]{0:T(128)} %bias_ref.1) | copy-start | bytes 196
  8.2 0.7 %copy-start.7 = (s32[32]{0:T(128)S(1)}, s32[32]{0:T(128)}, u32[]{:S(2)}) copy-start(s32[32]{0:T(128)} %lengths_ref.1) | copy-start | bytes 388
